TPU v7x, 32 devices: a whole 2x2x4 slice. The times are simulated.
32 devices in a mesh: sp: 16 (over z, y, x), tp: 2 (over core).
Axes of the slice: x: 2, y: 2, z: 4, core: 2. Of those that a mesh axis runs over, the one named last changes fastest.
Arguments:
- tokens: bfloat16 [4096, 2048], P('sp', 'tp'), may hold values from -6 to 6
- norm_gain: float32 [2048], replicated, may hold values from 0.1 to 1.9
- query_weight: bfloat16 [1024, 2048], P('tp'), may hold values from -0.125 to 0.125
- key_weight: bfloat16 [1024, 2048], P('tp'), may hold values from -0.125 to 0.125
- value_weight: bfloat16 [1024, 2048], P('tp'), may hold values from -0.125 to 0.125
- pool_weight: bfloat16 [1024, 2048], P('tp'), may hold values from -0.125 to 0.125
- query_gain: float32 [64], replicated, may hold values from 0.6 to 6
- key_gain: float32 [64], replicated, may hold values from 0.6 to 6
- cum_gate: float32 [4096, 16], P('sp', 'tp'), as said below
- out_pool_weight: bfloat16 [1024, 2048], P(None, 'tp'), may hold values from -0.1875 to 0.1875
- out_attn_weight: bfloat16 [1024, 2048], P(None, 'tp'), may hold values from -0.1875 to 0.1875
Outputs:
- mixed: bfloat16 [4096, 2048], P('sp', 'tp')
Inputs may be any that keep to these rules, and one draw needn't show every extreme that they name: `cum_gate`: in each head the values never rise along the positions.
All inputs are finite; a program needn't handle non-finite values.
Results may differ from a plain program's by a relative error of at most 0.005.
The roundings to bfloat16 on the way count: a program that leaves them out, or rounds other values in their place, can miss the bound.
Values may be sent and summed in bfloat16 or wider, within the bound.
A program may use at most 128 MiB of HBM per device.

v0:
```python
import math
import jax
import jax.numpy as jnp
from jax import lax
from jax.sharding import PartitionSpec as P

HEAD_DIM = 64
POOL_WIDTH = 1024
POOL_GROUPS = 4
epsilon = 1e-06
masked_fill = -1e30


def from_behind(value, axis, steps):
    count = lax.axis_size(axis)
    leading, last = (max(0, -steps), min(count, count - steps))
    return lax.ppermute(value, axis, [(source, source + steps) for source in range(leading, last)])


def rms_scale(values, gain):
    return values * lax.rsqrt(jnp.mean(values * values, axis=-1, keepdims=True) + epsilon) * gain


def block_partials(query_rows, query_pos, query_gate, key_rows, value_rows, key_pos, key_gate):
    logits = jnp.einsum("qhd,gkhd->qhgk", query_rows, key_rows, preferred_element_type=jnp.float32)
    logits = logits + query_gate[:, :, None, None] - jnp.transpose(key_gate, (2, 0, 1))[None]
    allowed = key_pos[None, None, :, :] <= query_pos[:, None, None, None]
    logits = jnp.where(allowed, logits, masked_fill)
    block_max = jnp.max(logits, axis=-1)
    weights = jnp.where(allowed, jnp.exp(logits - block_max[..., None]), 0.0)
    totals = jnp.sum(weights, axis=-1)
    numerator = jnp.einsum(
        "qhgk,gkhd->qhgd",
        weights.astype(jnp.bfloat16),
        value_rows,
        preferred_element_type=jnp.float32,
    )
    return (block_max, totals, numerator)


def merge_state(state, partials):
    run_max, run_den, run_acc = state
    block_max, totals, numerator = partials
    new_max = jnp.maximum(run_max, jnp.max(block_max, axis=-1))
    old_scale = jnp.exp(run_max - new_max)
    block_scale = jnp.exp(block_max - new_max[..., None])
    new_den = run_den * old_scale + jnp.sum(block_scale * totals, axis=-1)
    new_acc = run_acc * old_scale[..., None] + jnp.sum(block_scale[..., None] * numerator, axis=2)
    return (new_max, new_den, new_acc)


def empty_state(rows, heads_here):
    return (
        jnp.full((rows, heads_here), masked_fill, jnp.float32),
        jnp.zeros((rows, heads_here), jnp.float32),
        jnp.zeros((rows, heads_here, HEAD_DIM), jnp.float32),
    )


def per_device(
    tokens,
    norm_gain,
    query_weight,
    key_weight,
    value_weight,
    pool_weight,
    query_gain,
    key_gain,
    cum_gate,
    out_pool_weight,
    out_attn_weight,
):
    full_rows = lax.all_gather(tokens, "tp", axis=1, tiled=True)
    normed = rms_scale(full_rows.astype(jnp.float32), norm_gain).astype(jnp.bfloat16)
    length = full_rows.shape[0]
    heads_here = cum_gate.shape[1]
    offset = lax.axis_index("sp") * length

    def project(weight):
        return lax.dot_general(
            normed, weight, (((1,), (1,)), ((), ())), preferred_element_type=jnp.float32
        )

    query_heads = (
        rms_scale(project(query_weight).reshape(length, heads_here, HEAD_DIM), query_gain)
        * HEAD_DIM ** (-0.5)
    ).astype(jnp.bfloat16)
    key_heads = rms_scale(
        project(key_weight).reshape(length, heads_here, HEAD_DIM), key_gain
    ).astype(jnp.bfloat16)
    value_heads = project(value_weight).astype(jnp.bfloat16).reshape(length, heads_here, HEAD_DIM)
    pool_input = project(pool_weight).astype(jnp.bfloat16)
    reach = 2**POOL_GROUPS
    rim_rows = from_behind(pool_input[length - reach :], "sp", 1)
    extended = jnp.concatenate([rim_rows, pool_input], axis=0).astype(jnp.float32)
    prefix = jnp.cumsum(extended, axis=0)
    width_here = pool_input.shape[1]
    channel_ids = lax.axis_index("tp") * width_here + jnp.arange(width_here, dtype=jnp.int32)
    group_ids = channel_ids // (POOL_WIDTH // POOL_GROUPS)
    counts = (offset + jnp.arange(1, length + 1, dtype=jnp.int32)).astype(jnp.float32)[:, None]
    current = prefix[reach:]
    pooled_mean = jnp.zeros((length, width_here), jnp.float32)
    for group_index in range(POOL_GROUPS):
        window = 2 ** (group_index + 1)
        lagged = prefix[reach - window : reach - window + length]
        average = (current - lagged) / jnp.minimum(counts, float(window))
        pooled_mean = jnp.where(group_ids[None, :] == group_index, average, pooled_mean)
    pooled = (pooled_mean - extended[reach:]).astype(jnp.bfloat16)
    gate_all = lax.all_gather(cum_gate, "sp", axis=0, tiled=True)
    query_pos = offset + jnp.arange(length, dtype=jnp.int32)
    key_flat = key_heads.reshape(length, heads_here * HEAD_DIM)
    value_flat = value_heads.reshape(length, heads_here * HEAD_DIM)

    def absorb(carried, inputs):
        key_rows, value_rows, key_gate, key_pos = inputs
        partials = block_partials(
            query_heads, query_pos, cum_gate, key_rows, value_rows, key_pos, key_gate
        )
        return (merge_state(carried, partials), None)

    key_piece = lax.all_gather(key_flat, "sp", axis=0, tiled=True)
    value_piece = lax.all_gather(value_flat, "sp", axis=0, tiled=True)
    shards = key_piece.shape[0] // length
    grouping = math.gcd(shards, 8)
    turns = shards // grouping
    key_groups = key_piece.reshape(turns, grouping, length, heads_here, HEAD_DIM)
    value_groups = value_piece.reshape(turns, grouping, length, heads_here, HEAD_DIM)
    gate_groups = gate_all.reshape(turns, grouping, length, heads_here)
    pos_groups = jnp.arange(shards * length, dtype=jnp.int32).reshape(turns, grouping, length)
    result, _ = lax.scan(
        absorb, empty_state(length, heads_here), (key_groups, value_groups, gate_groups, pos_groups)
    )
    final_max, final_den, final_acc = result
    attended = (
        (final_acc / final_den[..., None])
        .reshape(length, heads_here * HEAD_DIM)
        .astype(jnp.bfloat16)
    )
    pool_full, attn_full = (
        lax.all_gather(pooled, "tp", axis=1, tiled=True),
        lax.all_gather(attended, "tp", axis=1, tiled=True),
    )
    output = jnp.dot(pool_full, out_pool_weight, preferred_element_type=jnp.float32) + jnp.dot(
        attn_full, out_attn_weight, preferred_element_type=jnp.float32
    )
    return output.astype(jnp.bfloat16)


def solution(mesh):
    return jax.shard_map(
        per_device,
        mesh=mesh,
        in_specs=(
            P("sp", "tp"),
            P(),
            P("tp", None),
            P("tp", None),
            P("tp", None),
            P("tp", None),
            P(),
            P(),
            P("sp", "tp"),
            P(None, "tp"),
            P(None, "tp"),
        ),
        out_specs=P("sp", "tp"),
        check_vma=False,
    )
```

profile of v0, /device:TPU:0, one launch (start us, length us, event | category | flops | bytes accessed | tf_op | source)
XLA Modules:
  0.0 260.2 jit_solution(4839599759511507353)
XLA Ops:
  6.5 0.7 all-gather.4.cloned.1.call-update
  7.3 0.7 mul.114
  8.0 12.6 %all-gather.4.cloned.1.call-done = bf16[256,2048]{1,0:T(8,128)(2,1)} async-done(((bf16[256,1024]{1,0:T(8,128)(2,1)}), bf16[256,2048]{1,0:T(8,128)(2,1)}) %all-gather.4.cloned.1.call-update) | async-done | bytes 1048592 | tf_op jit(solution)/shard_map/all_gather | solution.py:73
  20.7 1.5 fusion.24
  22.2 2.8 %fusion.50 = (f32[256,512]{1,0:T(8,128)S(1)}, f32[256,512]{1,0:T(8,128)}) fusion(bf16[512,2048]{1,0:T(8,128)(2,1)S(1)} %copy-done, bf16[256,2048]{1,0:T(8,128)(2,1)} %all-gather.4.cloned.1.call-done, f32[2048]{0:T(1024)} %param.14, f32[256]{0:T(256)S(1)} %add_rsqrt_fusion.2), kind=kOutput, calls=%fused_computation.93 | convolution fusion | flops 539099136 | bytes 4203520 | tf_op jit(solution)/shard_map/dot_general | solution.py:80
  26.0 0.8 multiply_convert_fusion.1
  26.9 3.0 %convolution_convert_fusion = bf16[256,512]{1,0:T(8,128)(2,1)} fusion(bf16[512,2048]{1,0:T(8,128)(2,1)} %param.17, bf16[256,2048]{1,0:T(8,128)(2,1)S(1)} %copy-done.4, f32[2048]{0:T(1024)S(1)} %copy-done.9, f32[256]{0:T(256)S(1)} %add_rsqrt_fusion.2), kind=kOutput, calls=%fused_computation.41 | convolution fusion | flops 539099136 | bytes 3417088 | tf_op jit(solution)/shard_map/dot_general | solution.py:80
  30.0 42.8 %all_gather.21 = f32[4096,8]{0,1:T(8,128)S(1)} all-gather(f32[256,8]{0,1:T(8,128)S(1)} %copy-done.6), channel_id=1, replica_groups=mesh['sp'=16,'tp'=2] {'sp'}, dimensions={0}, use_global_device_ids=true | all-gather | bytes 139264 | tf_op jit(solution)/shard_map/all_gather | solution.py:109
  72.9 2.5 convolution_convert_fusion.1
  75.4 1.3 collective-permute-start
  76.7 0.8 multiply_reduce_fusion.1
  77.7 0.7 collective-permute-done
  78.6 0.5 fusion.28
  80.2 2.5 all_gather.19
  82.7 0.7 fusion.51
  83.4 20.9 %all-gather.6.cloned.1.call-done = bf16[4096,512]{1,0:T(8,128)(2,1)} async-done(((bf16[256,512]{1,0:T(8,128)(2,1)}), bf16[4096,512]{1,0:T(8,128)(2,1)}) %all-gather.6.cloned.1.call-update) | async-done | bytes 4194320 | tf_op jit(solution)/shard_map/all_gather | solution.py:121
  104.3 11.2 %reshape.154 = bf16[2,8,256,8,64]{4,3,2,1,0:T(8,128)(2,1)} reshape(bf16[4096,512]{1,0:T(8,128)(2,1)} %all-gather.6.cloned.1.call-done) | data formatting | bytes 8388608 | tf_op jit(solution)/shard_map/reshape | solution.py:126
  115.5 9.8 %copy.42 = bf16[2,8,256,8,64]{2,4,1,3,0:T(8,128)(2,1)} copy(bf16[2,8,256,8,64]{4,3,2,1,0:T(8,128)(2,1)} %reshape.154) | data formatting | bytes 8388608
  125.3 56.0 %all-gather.8.cloned.1.call-done = bf16[4096,512]{1,0:T(8,128)(2,1)} async-done(((bf16[256,512]{1,0:T(8,128)(2,1)}), bf16[4096,512]{1,0:T(8,128)(2,1)}) %all-gather.8.cloned.1.call-update) | async-done | bytes 4194320 | tf_op jit(solution)/shard_map/all_gather | solution.py:122
  181.3 11.2 %reshape.155 = bf16[2,8,256,8,64]{4,3,2,1,0:T(8,128)(2,1)} reshape(bf16[4096,512]{1,0:T(8,128)(2,1)} %all-gather.8.cloned.1.call-done) | data formatting | bytes 8388608 | tf_op jit(solution)/shard_map/reshape | solution.py:127
  192.5 9.8 %copy.44 = bf16[2,8,256,8,64]{2,4,1,3,0:T(8,128)(2,1)} copy(bf16[2,8,256,8,64]{4,3,2,1,0:T(8,128)(2,1)} %reshape.155) | data formatting | bytes 8388608
  202.2 46.0 %while.15 = (s32[]{:T(128)}, f32[256,8]{0,1:T(8,128)S(1)}, f32[256,8]{0,1:T(8,128)S(1)}, f32[256,8,64]{0,2,1:T(8,128)S(1)}, s32[2,8,256]{2,1,0:T(8,128)S(1)}, /*...) while((s32[]{:T(128)}, f32[256,8]{0,1:T(8,128)S(1)}, ...), condition=%wide.region_11.12_spmd.clone, body=%wide.region_5.11_spmd.clone.sunk | while | flops 1122789632 | bytes 127101120 | solution.py:130
  202.8 6.9 %fusion.69 = (f32[256,8,8]{0,2,1:T(8,128)S(1)}, f32[256,8,8,256]{0,3,2,1:T(8,128)S(1)}) fusion(f32[8,8,256]{2,1,0:T(8,128)S(1)} %bitcast.72, f32[256,8]{0,1:T(8,128)S(1)} %get-tuple-element.297, bf16[256,8,64]{0,2,1:T(8,128)(2,1)S(1)} %get-tuple-element.296, bf16[2,8,256,8,64]{2,4,1,3,0:T(8,128)(2,1)} %get-tuple-element.295, s32[]{:T(128)S(6)} %copy.63, ...), kind=kOutput, calls=%fused_computation.92.clone.1 | convolution fusion | flops 553631744 | bytes 19800068 | tf_op jit(solution)/shard_map/while/body/eval_jaxpr/qhd,gkhd->qhgk/dot_general | solution.py:25
  209.7 4.8 %fusion.70 = (f32[256,8,8]{0,2,1:T(8,128)S(1)}, f32[256,8]{0,1:T(8,128)S(1)}) fusion(f32[256,8,8,256]{0,3,2,1:T(8,128)S(1)} %get-tuple-element.256, f32[256,8,8]{0,2,1:T(8,128)S(1)} %get-tuple-element.257, pred[256,8,256]{0,2,1:T(8,128)(4,1)S(1)} %broadcast_compare_fusion.6), kind=kLoop, calls=%fused_computation.6.clone.1 | loop fusion | flops 16758784 | bytes 17440768 | tf_op jit(solution)/shard_map/while/body/eval_jaxpr/reduce_sum | solution.py:31
  214.5 0.9 copy-done.2
  215.5 9.5 %fusion.72 = f32[256,8,64]{0,2,1:T(8,128)S(1)} fusion(f32[256,8,8,256]{0,3,2,1:T(8,128)} %copy-done.2, f32[256,8,8]{0,2,1:T(8,128)S(1)} %get-tuple-element.257, pred[256,8,256]{0,2,1:T(8,128)(4,1)S(1)} %broadcast_compare_fusion.6, bf16[2,8,256,8,64]{2,4,1,3,0:T(8,128)(2,1)} %get-tuple-element.299, s32[]{:T(128)S(6)} %copy.63, ...), kind=kOutput, calls=%fused_computation.12.clone.1 | convolution fusion | flops 551419904 | bytes 20054020 | tf_op jit(solution)/shard_map/while/body/eval_jaxpr/qhgk,gkhd->qhgd/dot_general | solution.py:32
  225.8 6.9 %fusion.69 = (f32[256,8,8]{0,2,1:T(8,128)S(1)}, f32[256,8,8,256]{0,3,2,1:T(8,128)S(1)}) fusion(f32[8,8,256]{2,1,0:T(8,128)S(1)} %bitcast.72, f32[256,8]{0,1:T(8,128)S(1)} %get-tuple-element.297, bf16[256,8,64]{0,2,1:T(8,128)(2,1)S(1)} %get-tuple-element.296, bf16[2,8,256,8,64]{2,4,1,3,0:T(8,128)(2,1)} %get-tuple-element.295, s32[]{:T(128)S(6)} %copy.63, ...), kind=kOutput, calls=%fused_computation.92.clone.1 | convolution fusion | flops 553631744 | bytes 19800068 | tf_op jit(solution)/shard_map/while/body/eval_jaxpr/qhd,gkhd->qhgk/dot_general | solution.py:25
  232.7 4.8 %fusion.70 = (f32[256,8,8]{0,2,1:T(8,128)S(1)}, f32[256,8]{0,1:T(8,128)S(1)}) fusion(f32[256,8,8,256]{0,3,2,1:T(8,128)S(1)} %get-tuple-element.256, f32[256,8,8]{0,2,1:T(8,128)S(1)} %get-tuple-element.257, pred[256,8,256]{0,2,1:T(8,128)(4,1)S(1)} %broadcast_compare_fusion.6), kind=kLoop, calls=%fused_computation.6.clone.1 | loop fusion | flops 16758784 | bytes 17440768 | tf_op jit(solution)/shard_map/while/body/eval_jaxpr/reduce_sum | solution.py:31
  237.5 0.9 copy-done.2
  238.5 9.5 %fusion.72 = f32[256,8,64]{0,2,1:T(8,128)S(1)} fusion(f32[256,8,8,256]{0,3,2,1:T(8,128)} %copy-done.2, f32[256,8,8]{0,2,1:T(8,128)S(1)} %get-tuple-element.257, pred[256,8,256]{0,2,1:T(8,128)(4,1)S(1)} %broadcast_compare_fusion.6, bf16[2,8,256,8,64]{2,4,1,3,0:T(8,128)(2,1)} %get-tuple-element.299, s32[]{:T(128)S(6)} %copy.63, ...), kind=kOutput, calls=%fused_computation.12.clone.1 | convolution fusion | flops 551419904 | bytes 20054020 | tf_op jit(solution)/shard_map/while/body/eval_jaxpr/qhgk,gkhd->qhgd/dot_general | solution.py:32
  248.3 2.3 all_gather.23
  250.6 3.1 %fusion.27 = bf16[256,1024]{1,0:T(8,128)(2,1)} fusion(f32[256,1024]{1,0:T(8,128)S(1)} %fusion.51, bf16[256,1024]{0,1:T(8,128)(2,1)S(1)} %all_gather.23, bf16[1024,1024]{1,0:T(8,128)(2,1)} %param.23), kind=kOutput, calls=%fused_computation.40 | convolution fusion | flops 537395200 | bytes 4194304 | tf_op jit(solution)/shard_map/dot_general | solution.py:143
  (71 shorter events, 4.2 us)
Async XLA Ops:
  6.5 15.6 %copy-start = (bf16[512,2048]{1,0:T(8,128)(2,1)S(1)}, bf16[512,2048]{1,0:T(8,128)(2,1)}, u32[]{:S(2)}) copy-start(bf16[512,2048]{1,0:T(8,128)(2,1)} %param.16) | copy-start | bytes 6291460
  6.5 14.1 %all-gather.4.cloned.1.call-start = ((), (), s32[]{:S(2)}) async-start(), calls=%async_computation | async-start | bytes 1572864 | tf_op jit(solution)/shard_map/all_gather | solution.py:73
  7.3 97.0 %all-gather.6.cloned.1.call-start = ((), (), s32[]{:S(2)}) async-start(), calls=%async_computation.1 | async-start | bytes 4456448 | tf_op jit(solution)/shard_map/all_gather | solution.py:121
  25.0 1.0 copy-start.5
  25.2 1.7 copy-start.4
  25.2 1.7 copy-start.9
  26.8 3.2 %copy-start.6 = (f32[256,8]{0,1:T(8,128)S(1)}, f32[256,8]{0,1:T(8,128)}, u32[]{:S(2)}) copy-start(f32[256,8]{0,1:T(8,128)} %param.21) | copy-start | bytes 24580
  26.9 154.4 %all-gather.8.cloned.1.call-start = ((), (), s32[]{:S(2)}) async-start(), calls=%async_computation.2 | async-start | bytes 4456448 | tf_op jit(solution)/shard_map/all_gather | solution.py:122
  72.9 3.8 %copy-start.8 = (bf16[512,2048]{1,0:T(8,128)(2,1)S(1)}, bf16[512,2048]{1,0:T(8,128)(2,1)}, u32[]{:S(2)}) copy-start(bf16[512,2048]{1,0:T(8,128)(2,1)} %param.15) | copy-start | bytes 6291460
  75.4 2.2 copy-start.7
  75.4 3.0 %collective-permute-start = (bf16[16,512]{1,0:T(8,128)(2,1)S(1)}, bf16[16,512]{1,0:T(8,128)(2,1)S(1)}, u32[]{:S(2)}, u32[]{:S(2)}) collective-permute-start(bf16[16,512]{1,0:T(8,128)(2,1)S(1)} %slice.42), channel_id=1, source_target_pairs={{0,2},{2,4},{4,6},{6,8},{8,10},{10,12},{12,14},{14,16},{16,18},{18... | collective-permute-start | bytes 49160 | tf_op jit(solution)/shard_map/ppermute | solution.py:17
  79.7 3.0 %copy-start.3 = (bf16[1024,1024]{1,0:T(8,128)(2,1)S(1)}, bf16[1024,1024]{1,0:T(8,128)(2,1)}, u32[]{:S(2)}) copy-start(bf16[1024,1024]{1,0:T(8,128)(2,1)} %param.22) | copy-start | bytes 6291460
  209.7 5.7 %copy-start.2 = (f32[256,8,8,256]{0,3,2,1:T(8,128)}, f32[256,8,8,256]{0,3,2,1:T(8,128)S(1)}, u32[]{:S(2)}) copy-start(f32[256,8,8,256]{0,3,2,1:T(8,128)S(1)} %get-tuple-element.256) | copy-start | bytes 50331652 | tf_op jit(solution)/shard_map/while
  232.7 5.7 %copy-start.2 = (f32[256,8,8,256]{0,3,2,1:T(8,128)}, f32[256,8,8,256]{0,3,2,1:T(8,128)S(1)}, u32[]{:S(2)}) copy-start(f32[256,8,8,256]{0,3,2,1:T(8,128)S(1)} %get-tuple-element.256) | copy-start | bytes 50331652 | tf_op jit(solution)/shard_map/while
  248.2 5.4 %copy-start.1 = (bf16[512,2048]{1,0:T(8,128)(2,1)S(1)}, bf16[512,2048]{1,0:T(8,128)(2,1)}, u32[]{:S(2)}) copy-start(bf16[512,2048]{1,0:T(8,128)(2,1)} %param.16) | copy-start | bytes 6291460
Sparse Core Ops, SparseCore 0:
  8.9 11.7 all-gather.3
  27.0 77.2 all-gather.5
  107.1 74.1 all-gather.7
where the time goes:
time: 262 us; the launch traced here: 260 us
  waiting for transfers between devices  90.9 us (35%)
  blocking collectives  47.6 us (18%)
  local copies, waits for them, and re-layouts  45.9 us (18%)
  matrix products  45.8 us (17%)
  other arithmetic  15 us (6%)
  between operations  13.4 us (5%)
    all_gather x1, waiting for transfers between devices, per_device(): value_piece = lax.all_gather(value_flat, 'sp', axis=0, tiled=True)  56 us
    all_gather x1, blocking collectives, per_device(): gate_all = lax.all_gather(cum_gate, 'sp', axis=0, tiled=True)  42.8 us
    all_gather x1, waiting for transfers between devices, per_device(): key_piece = lax.all_gather(key_flat, 'sp', axis=0, tiled=True)  20.9 us
    unnamed x20, local copies, waits for them, and re-layouts  20.1 us
    dot_general x2, matrix products, block_partials(): jnp.einsum('qhgk,gkhd->qhgd', weights.astype(jnp.bfloat16), value_rows, p...  19 us
    dot_general x2, matrix products, block_partials(): jnp.einsum('qhd,gkhd->qhgk', query_rows, key_rows, preferred_element_type...  13.8 us
    all_gather x1, waiting for transfers between devices, per_device(): full_rows = lax.all_gather(tokens, 'tp', axis=1, tiled=True)  12.6 us
    reshape x1, local copies, waits for them, and re-layouts, per_device(): key_piece.reshape(turns, grouping, length, heads_here, HEAD_DIM)  11.2 us
  transfers between devices with their start and end apart: 4, of which 4 were waited for; matrix products, arithmetic and copies ran while one was open for 12% of the time, Pallas kernels for 0%

commit v1 on v0

--- a/solution.py
+++ b/solution.py
@@ -119,7 +119,12 @@
         return (merge_state(carried, partials), None)
 
     key_piece = lax.all_gather(key_flat, "sp", axis=0, tiled=True)
-    value_piece = lax.all_gather(value_flat, "sp", axis=0, tiled=True)
+    ring = [value_flat]
+    for hop in range(15):
+        ring.append(lax.ppermute(ring[-1], "sp", [(dev, (dev + 1) % 16) for dev in range(16)]))
+    value_piece = jnp.roll(
+        jnp.concatenate(ring[::-1], axis=0), (lax.axis_index("sp") + 1) * ring[0].shape[0], axis=0
+    )
     shards = key_piece.shape[0] // length
     grouping = math.gcd(shards, 8)
     turns = shards // grouping

time: 262 us -> 340 us (1.30)
  waiting for transfers between devices: 90.9 us -> 147 us
  local copies, waits for them, and re-layouts: 45.9 us -> 58.4 us
  matrix products: 45.8 us -> 50.7 us
    ppermute x0 -> x15, waiting for transfers between devices: none -> 133 us  [per_device(): lax.ppermute(ring[-1], 'sp', [(dev, (dev + 1) % 16) for dev in range(16)])]
    all_gather x1 -> x0, waiting for transfers between devices: 56 us -> none  [per_device(): value_piece = lax.all_gather(value_flat, 'sp', axis=0, tiled=True)]
    all_gather x1, waiting for transfers between devices: 20.9 us -> 0.01 us  [per_device(): key_piece = lax.all_gather(key_flat, 'sp', axis=0, tiled=True)]
    unnamed x20 -> x89, local copies, waits for them, and re-layouts: 20.1 us -> 29.3 us
  transfers between devices with their start and end apart: 4 -> 18, of which waited for: 4 -> 15; matrix products, arithmetic and copies ran while one was open for 12% -> 14% of each run, Pallas kernels for 0% -> 0%
where the time goes in v1:
time: 340 us; the launch traced here: 338 us
  waiting for transfers between devices  147 us (43%)
  local copies, waits for them, and re-layouts  58.4 us (17%)
  matrix products  50.7 us (15%)
  blocking collectives  48.2 us (14%)
  other arithmetic  15.8 us (5%)
  between operations  14.1 us (4%)
  starting transfers between devices  3.54 us (1%)
    ppermute x15, waiting for transfers between devices, per_device(): lax.ppermute(ring[-1], 'sp', [(dev, (dev + 1) % 16) for dev in range(16)])  133 us
    all_gather x1, blocking collectives, per_device(): gate_all = lax.all_gather(cum_gate, 'sp', axis=0, tiled=True)  43.5 us
    unnamed x89, local copies, waits for them, and re-layouts  29.3 us
    dot_general x2, matrix products, block_partials(): jnp.einsum('qhgk,gkhd->qhgd', weights.astype(jnp.bfloat16), value_rows, p...  19 us
    dot_general x2, matrix products, block_partials(): jnp.einsum('qhd,gkhd->qhgk', query_rows, key_rows, preferred_element_type...  13.9 us
    all_gather x1, waiting for transfers between devices, per_device(): full_rows = lax.all_gather(tokens, 'tp', axis=1, tiled=True)  13.4 us
    reshape x1, local copies, waits for them, and re-layouts, per_device(): key_piece.reshape(turns, grouping, length, heads_here, HEAD_DIM)  11.2 us
    reshape x1, local copies, waits for them, and re-layouts, per_device(): value_piece.reshape(turns, grouping, length, heads_here, HEAD_DIM)  11.2 us
  transfers between devices with their start and end apart: 18, of which 15 were waited for; matrix products, arithmetic and copies ran while one was open for 14% of the time, Pallas kernels for 0%

profile of v1, /device:TPU:0, one launch (start us, length us, event | category | flops | bytes accessed | tf_op | source)
XLA Modules:
  0.0 338.4 jit_solution(18023697523310996248)
XLA Ops:
  7.3 13.4 %all-gather.3.cloned.1.call-done = bf16[256,2048]{1,0:T(8,128)(2,1)} async-done(((bf16[256,1024]{1,0:T(8,128)(2,1)}), bf16[256,2048]{1,0:T(8,128)(2,1)}) %all-gather.3.cloned.1.call-update) | async-done | bytes 1048592 | tf_op jit(solution)/shard_map/all_gather | solution.py:73
  27.3 10.4 %collective-permute-done.1 = bf16[256,512]{1,0:T(8,128)(2,1)S(1)} collective-permute-done((bf16[256,512]{1,0:T(8,128)(2,1)S(1)}, bf16[256,512]{1,0:T(8,128)(2,1)S(1)}, u32[]{:S(2)}, u32[]{:S(2)}) %collective-permute-start.1) | collective-permute-done | bytes 262176 | tf_op jit(solution)/shard_map/ppermute | solution.py:124
  38.5 11.3 %collective-permute-done.2 = bf16[256,512]{1,0:T(8,128)(2,1)S(1)} collective-permute-done((bf16[256,512]{1,0:T(8,128)(2,1)S(1)}, bf16[256,512]{1,0:T(8,128)(2,1)S(1)}, u32[]{:S(2)}, u32[]{:S(2)}) %collective-permute-start.2) | collective-permute-done | bytes 262176 | tf_op jit(solution)/shard_map/ppermute | solution.py:124
  50.5 9.7 %collective-permute-done.3 = bf16[256,512]{1,0:T(8,128)(2,1)S(1)} collective-permute-done((bf16[256,512]{1,0:T(8,128)(2,1)S(1)}, bf16[256,512]{1,0:T(8,128)(2,1)S(1)}, u32[]{:S(2)}, u32[]{:S(2)}) %collective-permute-start.3) | collective-permute-done | bytes 262176 | tf_op jit(solution)/shard_map/ppermute | solution.py:124
  60.3 2.9 fusion.50
  64.4 5.8 %collective-permute-done.4 = bf16[256,512]{1,0:T(8,128)(2,1)S(1)} collective-permute-done((bf16[256,512]{1,0:T(8,128)(2,1)S(1)}, bf16[256,512]{1,0:T(8,128)(2,1)S(1)}, u32[]{:S(2)}, u32[]{:S(2)}) %collective-permute-start.4) | collective-permute-done | bytes 262176 | tf_op jit(solution)/shard_map/ppermute | solution.py:124
  70.6 9.7 %collective-permute-done.5 = bf16[256,512]{1,0:T(8,128)(2,1)S(1)} collective-permute-done((bf16[256,512]{1,0:T(8,128)(2,1)S(1)}, bf16[256,512]{1,0:T(8,128)(2,1)S(1)}, u32[]{:S(2)}, u32[]{:S(2)}) %collective-permute-start.5) | collective-permute-done | bytes 262176 | tf_op jit(solution)/shard_map/ppermute | solution.py:124
  81.1 9.2 %collective-permute-done.6 = bf16[256,512]{1,0:T(8,128)(2,1)S(1)} collective-permute-done((bf16[256,512]{1,0:T(8,128)(2,1)S(1)}, bf16[256,512]{1,0:T(8,128)(2,1)S(1)}, u32[]{:S(2)}, u32[]{:S(2)}) %collective-permute-start.6) | collective-permute-done | bytes 262176 | tf_op jit(solution)/shard_map/ppermute | solution.py:124
  90.4 16.8 %collective-permute-done.7 = bf16[256,512]{1,0:T(8,128)(2,1)S(1)} collective-permute-done((bf16[256,512]{1,0:T(8,128)(2,1)S(1)}, bf16[256,512]{1,0:T(8,128)(2,1)S(1)}, u32[]{:S(2)}, u32[]{:S(2)}) %collective-permute-start.7) | collective-permute-done | bytes 262176 | tf_op jit(solution)/shard_map/ppermute | solution.py:124
  107.2 43.5 %all_gather.18 = f32[4096,8]{0,1:T(8,128)S(1)} all-gather(f32[256,8]{0,1:T(8,128)S(1)} %copy-done.26), channel_id=1, replica_groups=mesh['sp'=16,'tp'=2] {'sp'}, dimensions={0}, use_global_device_ids=true | all-gather | bytes 139264 | tf_op jit(solution)/shard_map/all_gather | solution.py:109
  150.9 2.7 convolution_convert_fusion.1
  155.2 7.6 %collective-permute-done.9 = bf16[256,512]{1,0:T(8,128)(2,1)S(1)} collective-permute-done((bf16[256,512]{1,0:T(8,128)(2,1)S(1)}, bf16[256,512]{1,0:T(8,128)(2,1)S(1)}, u32[]{:S(2)}, u32[]{:S(2)}) %collective-permute-start.9) | collective-permute-done | bytes 262176 | tf_op jit(solution)/shard_map/ppermute | solution.py:124
  162.8 2.8 multiply_reduce_fusion.1
  165.7 9.7 %collective-permute-done.10 = bf16[256,512]{1,0:T(8,128)(2,1)S(1)} collective-permute-done((bf16[256,512]{1,0:T(8,128)(2,1)S(1)}, bf16[256,512]{1,0:T(8,128)(2,1)S(1)}, u32[]{:S(2)}, u32[]{:S(2)}) %collective-permute-start.10) | collective-permute-done | bytes 262176 | tf_op jit(solution)/shard_map/ppermute | solution.py:124
  176.5 9.6 %collective-permute-done.11 = bf16[256,512]{1,0:T(8,128)(2,1)} collective-permute-done((bf16[256,512]{1,0:T(8,128)(2,1)S(1)}, bf16[256,512]{1,0:T(8,128)(2,1)}, u32[]{:S(2)}, u32[]{:S(2)}) %collective-permute-start.11) | collective-permute-done | bytes 262176 | tf_op jit(solution)/shard_map/ppermute | solution.py:124
  186.7 9.7 %collective-permute-done.12 = bf16[256,512]{1,0:T(8,128)(2,1)} collective-permute-done((bf16[256,512]{1,0:T(8,128)(2,1)}, bf16[256,512]{1,0:T(8,128)(2,1)}, u32[]{:S(2)}, u32[]{:S(2)}) %collective-permute-start.12) | collective-permute-done | bytes 262176 | tf_op jit(solution)/shard_map/ppermute | solution.py:124
  196.9 9.7 %collective-permute-done.13 = bf16[256,512]{1,0:T(8,128)(2,1)S(1)} collective-permute-done((bf16[256,512]{1,0:T(8,128)(2,1)}, bf16[256,512]{1,0:T(8,128)(2,1)S(1)}, u32[]{:S(2)}, u32[]{:S(2)}) %collective-permute-start.13) | collective-permute-done | bytes 262176 | tf_op jit(solution)/shard_map/ppermute | solution.py:124
  209.4 7.5 %collective-permute-done.14 = bf16[256,512]{1,0:T(8,128)(2,1)S(1)} collective-permute-done((bf16[256,512]{1,0:T(8,128)(2,1)S(1)}, bf16[256,512]{1,0:T(8,128)(2,1)S(1)}, u32[]{:S(2)}, u32[]{:S(2)}) %collective-permute-start.14) | collective-permute-done | bytes 262176 | tf_op jit(solution)/shard_map/ppermute | solution.py:124
  217.0 3.3 fusion.51
  220.3 6.6 %collective-permute-done.15 = bf16[256,512]{1,0:T(8,128)(2,1)S(1)} collective-permute-done((bf16[256,512]{1,0:T(8,128)(2,1)S(1)}, bf16[256,512]{1,0:T(8,128)(2,1)S(1)}, u32[]{:S(2)}, u32[]{:S(2)}) %collective-permute-start.15) | collective-permute-done | bytes 262176 | tf_op jit(solution)/shard_map/ppermute | solution.py:124
  237.7 11.2 %reshape.155 = bf16[2,8,256,8,64]{4,3,2,1,0:T(8,128)(2,1)} reshape(bf16[4096,512]{1,0:T(8,128)(2,1)} %constant_dynamic-slice_fusion.1) | data formatting | bytes 8388608 | tf_op jit(solution)/shard_map/reshape | solution.py:132
  248.9 9.7 %copy.43 = bf16[2,8,256,8,64]{2,4,1,3,0:T(8,128)(2,1)} copy(bf16[2,8,256,8,64]{4,3,2,1,0:T(8,128)(2,1)} %reshape.155) | data formatting | bytes 8388608
  258.6 11.2 %reshape.154 = bf16[2,8,256,8,64]{4,3,2,1,0:T(8,128)(2,1)} reshape(bf16[4096,512]{1,0:T(8,128)(2,1)} %all-gather.5.cloned.1.call-done) | data formatting | bytes 8388608 | tf_op jit(solution)/shard_map/reshape | solution.py:131
  269.9 9.8 %copy.41 = bf16[2,8,256,8,64]{2,4,1,3,0:T(8,128)(2,1)} copy(bf16[2,8,256,8,64]{4,3,2,1,0:T(8,128)(2,1)} %reshape.154) | data formatting | bytes 8388608
  279.7 46.1 %while.15 = (s32[]{:T(128)}, f32[256,8]{0,1:T(8,128)S(1)}, f32[256,8]{0,1:T(8,128)S(1)}, f32[256,8,64]{0,2,1:T(8,128)S(1)}, s32[2,8,256]{2,1,0:T(8,128)S(1)}, /*...) while((s32[]{:T(128)}, f32[256,8]{0,1:T(8,128)S(1)}, ...), condition=%wide.region_11.12_spmd.clone, body=%wide.region_5.11_spmd.clone.sunk | while | flops 1122789632 | bytes 127101120 | solution.py:135
  280.2 7.0 %fusion.69 = (f32[256,8,8]{0,2,1:T(8,128)S(1)}, f32[256,8,8,256]{0,3,2,1:T(8,128)S(1)}) fusion(f32[8,8,256]{2,1,0:T(8,128)S(1)} %bitcast.72, f32[256,8]{0,1:T(8,128)S(1)} %get-tuple-element.297, bf16[256,8,64]{0,2,1:T(8,128)(2,1)S(1)} %get-tuple-element.296, bf16[2,8,256,8,64]{2,4,1,3,0:T(8,128)(2,1)} %get-tuple-element.295, s32[]{:T(128)S(6)} %copy.93, ...), kind=kOutput, calls=%fused_computation.125.clone.1 | convolution fusion | flops 553631744 | bytes 19800068 | tf_op jit(solution)/shard_map/while/body/eval_jaxpr/qhd,gkhd->qhgk/dot_general | solution.py:25
  287.2 4.8 %fusion.70 = (f32[256,8,8]{0,2,1:T(8,128)S(1)}, f32[256,8]{0,1:T(8,128)S(1)}) fusion(f32[256,8,8,256]{0,3,2,1:T(8,128)S(1)} %get-tuple-element.256, f32[256,8,8]{0,2,1:T(8,128)S(1)} %get-tuple-element.257, pred[256,8,256]{0,2,1:T(8,128)(4,1)S(1)} %broadcast_compare_fusion.6), kind=kLoop, calls=%fused_computation.6.clone.1 | loop fusion | flops 16758784 | bytes 17440768 | tf_op jit(solution)/shard_map/while/body/eval_jaxpr/reduce_sum | solution.py:31
  293.0 9.5 %fusion.72 = f32[256,8,64]{0,2,1:T(8,128)S(1)} fusion(f32[256,8,8,256]{0,3,2,1:T(8,128)} %copy-done.2, f32[256,8,8]{0,2,1:T(8,128)S(1)} %get-tuple-element.257, pred[256,8,256]{0,2,1:T(8,128)(4,1)S(1)} %broadcast_compare_fusion.6, bf16[2,8,256,8,64]{2,4,1,3,0:T(8,128)(2,1)} %get-tuple-element.299, s32[]{:T(128)S(6)} %copy.93, ...), kind=kOutput, calls=%fused_computation.12.clone.1 | convolution fusion | flops 551419904 | bytes 20054020 | tf_op jit(solution)/shard_map/while/body/eval_jaxpr/qhgk,gkhd->qhgd/dot_general | solution.py:32
  303.3 7.0 %fusion.69 = (f32[256,8,8]{0,2,1:T(8,128)S(1)}, f32[256,8,8,256]{0,3,2,1:T(8,128)S(1)}) fusion(f32[8,8,256]{2,1,0:T(8,128)S(1)} %bitcast.72, f32[256,8]{0,1:T(8,128)S(1)} %get-tuple-element.297, bf16[256,8,64]{0,2,1:T(8,128)(2,1)S(1)} %get-tuple-element.296, bf16[2,8,256,8,64]{2,4,1,3,0:T(8,128)(2,1)} %get-tuple-element.295, s32[]{:T(128)S(6)} %copy.93, ...), kind=kOutput, calls=%fused_computation.125.clone.1 | convolution fusion | flops 553631744 | bytes 19800068 | tf_op jit(solution)/shard_map/while/body/eval_jaxpr/qhd,gkhd->qhgk/dot_general | solution.py:25
  310.2 4.8 %fusion.70 = (f32[256,8,8]{0,2,1:T(8,128)S(1)}, f32[256,8]{0,1:T(8,128)S(1)}) fusion(f32[256,8,8,256]{0,3,2,1:T(8,128)S(1)} %get-tuple-element.256, f32[256,8,8]{0,2,1:T(8,128)S(1)} %get-tuple-element.257, pred[256,8,256]{0,2,1:T(8,128)(4,1)S(1)} %broadcast_compare_fusion.6), kind=kLoop, calls=%fused_computation.6.clone.1 | loop fusion | flops 16758784 | bytes 17440768 | tf_op jit(solution)/shard_map/while/body/eval_jaxpr/reduce_sum | solution.py:31
  316.0 9.5 %fusion.72 = f32[256,8,64]{0,2,1:T(8,128)S(1)} fusion(f32[256,8,8,256]{0,3,2,1:T(8,128)} %copy-done.2, f32[256,8,8]{0,2,1:T(8,128)S(1)} %get-tuple-element.257, pred[256,8,256]{0,2,1:T(8,128)(4,1)S(1)} %broadcast_compare_fusion.6, bf16[2,8,256,8,64]{2,4,1,3,0:T(8,128)(2,1)} %get-tuple-element.299, s32[]{:T(128)S(6)} %copy.93, ...), kind=kOutput, calls=%fused_computation.12.clone.1 | convolution fusion | flops 551419904 | bytes 20054020 | tf_op jit(solution)/shard_map/while/body/eval_jaxpr/qhgk,gkhd->qhgd/dot_general | solution.py:32
  328.1 3.4 fusion.27
  (169 shorter events, 34.2 us)
Async XLA Ops:
  6.5 53.7 %copy-start = (bf16[512,2048]{1,0:T(8,128)(2,1)S(1)}, bf16[512,2048]{1,0:T(8,128)(2,1)}, u32[]{:S(2)}) copy-start(bf16[512,2048]{1,0:T(8,128)(2,1)} %param.16) | copy-start | bytes 6291460
  6.5 144.3 %copy-start.28 = (f32[2048]{0:T(1024)S(1)}, f32[2048]{0:T(1024)}, u32[]{:S(2)}) copy-start(f32[2048]{0:T(1024)} %param.14) | copy-start | bytes 24580
  6.5 100.7 %copy-start.26 = (f32[256,8]{0,1:T(8,128)S(1)}, f32[256,8]{0,1:T(8,128)}, u32[]{:S(2)}) copy-start(f32[256,8]{0,1:T(8,128)} %param.21) | copy-start | bytes 24580
  6.5 14.1 %all-gather.3.cloned.1.call-start = ((), (), s32[]{:S(2)}) async-start(), calls=%async_computation | async-start | bytes 1572864 | tf_op jit(solution)/shard_map/all_gather | solution.py:73
  7.3 251.4 %all-gather.5.cloned.1.call-start = ((), (), s32[]{:S(2)}) async-start(), calls=%async_computation.1 | async-start | bytes 4456448 | tf_op jit(solution)/shard_map/all_gather | solution.py:121
  25.6 12.2 %collective-permute-start.1 = (bf16[256,512]{1,0:T(8,128)(2,1)S(1)}, bf16[256,512]{1,0:T(8,128)(2,1)S(1)}, u32[]{:S(2)}, u32[]{:S(2)}) collective-permute-start(bf16[256,512]{1,0:T(8,128)(2,1)S(1)} %convolution_convert_fusion), channel_id=1, source_target_pairs={{0,2},{2,4},{4,6},{6,8},{8,10},{10,12},{12,14},{14,16},{16,18},{18... | collective-permute-start | bytes 786440 | tf_op jit(solution)/shard_map/ppermute | solution.py:124
  38.5 11.3 %collective-permute-start.2 = (bf16[256,512]{1,0:T(8,128)(2,1)S(1)}, bf16[256,512]{1,0:T(8,128)(2,1)S(1)}, u32[]{:S(2)}, u32[]{:S(2)}) collective-permute-start(bf16[256,512]{1,0:T(8,128)(2,1)S(1)} %collective-permute-done.1), channel_id=1, source_target_pairs={{0,2},{2,4},{4,6},{6,8},{8,10},{10,12},{12,14},{14,16},{16,18},{18... | collective-permute-start | bytes 786440 | tf_op jit(solution)/shard_map/ppermute | solution.py:124
  49.8 40.5 %copy-start.7 = (bf16[256,512]{1,0:T(8,128)(2,1)}, bf16[256,512]{1,0:T(8,128)(2,1)S(1)}, u32[]{:S(2)}) copy-start(bf16[256,512]{1,0:T(8,128)(2,1)S(1)} %collective-permute-done.2) | copy-start | bytes 786436
  49.8 10.5 %collective-permute-start.3 = (bf16[256,512]{1,0:T(8,128)(2,1)S(1)}, bf16[256,512]{1,0:T(8,128)(2,1)S(1)}, u32[]{:S(2)}, u32[]{:S(2)}) collective-permute-start(bf16[256,512]{1,0:T(8,128)(2,1)S(1)} %collective-permute-done.2), channel_id=1, source_target_pairs={{0,2},{2,4},{4,6},{6,8},{8,10},{10,12},{12,14},{14,16},{16,18},{18... | collective-permute-start | bytes 786440 | tf_op jit(solution)/shard_map/ppermute | solution.py:124
  60.3 10.0 %collective-permute-start.4 = (bf16[256,512]{1,0:T(8,128)(2,1)S(1)}, bf16[256,512]{1,0:T(8,128)(2,1)S(1)}, u32[]{:S(2)}, u32[]{:S(2)}) collective-permute-start(bf16[256,512]{1,0:T(8,128)(2,1)S(1)} %collective-permute-done.3), channel_id=1, source_target_pairs={{0,2},{2,4},{4,6},{6,8},{8,10},{10,12},{12,14},{14,16},{16,18},{18... | collective-permute-start | bytes 786440 | tf_op jit(solution)/shard_map/ppermute | solution.py:124
  63.2 112.2 %copy-start.27 = (f32[64]{0:T(128)S(1)}, f32[64]{0:T(128)}, u32[]{:S(2)}) copy-start(f32[64]{0:T(128)} %param.19) | copy-start | bytes 772
  70.2 106.0 %copy-start.11 = (bf16[256,512]{1,0:T(8,128)(2,1)}, bf16[256,512]{1,0:T(8,128)(2,1)S(1)}, u32[]{:S(2)}) copy-start(bf16[256,512]{1,0:T(8,128)(2,1)S(1)} %collective-permute-done.4) | copy-start | bytes 786436
  70.2 10.0 %collective-permute-start.5 = (bf16[256,512]{1,0:T(8,128)(2,1)S(1)}, bf16[256,512]{1,0:T(8,128)(2,1)S(1)}, u32[]{:S(2)}, u32[]{:S(2)}) collective-permute-start(bf16[256,512]{1,0:T(8,128)(2,1)S(1)} %collective-permute-done.4), channel_id=1, source_target_pairs={{0,2},{2,4},{4,6},{6,8},{8,10},{10,12},{12,14},{14,16},{16,18},{18... | collective-permute-start | bytes 786440 | tf_op jit(solution)/shard_map/ppermute | solution.py:124
  80.2 96.2 %copy-start.13 = (bf16[256,512]{1,0:T(8,128)(2,1)}, bf16[256,512]{1,0:T(8,128)(2,1)S(1)}, u32[]{:S(2)}) copy-start(bf16[256,512]{1,0:T(8,128)(2,1)S(1)} %collective-permute-done.5) | copy-start | bytes 786436
  80.2 10.1 %collective-permute-start.6 = (bf16[256,512]{1,0:T(8,128)(2,1)S(1)}, bf16[256,512]{1,0:T(8,128)(2,1)S(1)}, u32[]{:S(2)}, u32[]{:S(2)}) collective-permute-start(bf16[256,512]{1,0:T(8,128)(2,1)S(1)} %collective-permute-done.5), channel_id=1, source_target_pairs={{0,2},{2,4},{4,6},{6,8},{8,10},{10,12},{12,14},{14,16},{16,18},{18... | collective-permute-start | bytes 786440 | tf_op jit(solution)/shard_map/ppermute | solution.py:124
  90.3 86.0 %copy-start.15 = (bf16[256,512]{1,0:T(8,128)(2,1)}, bf16[256,512]{1,0:T(8,128)(2,1)S(1)}, u32[]{:S(2)}) copy-start(bf16[256,512]{1,0:T(8,128)(2,1)S(1)} %collective-permute-done.6) | copy-start | bytes 786436
  90.3 16.9 %collective-permute-start.7 = (bf16[256,512]{1,0:T(8,128)(2,1)S(1)}, bf16[256,512]{1,0:T(8,128)(2,1)S(1)}, u32[]{:S(2)}, u32[]{:S(2)}) collective-permute-start(bf16[256,512]{1,0:T(8,128)(2,1)S(1)} %collective-permute-done.6), channel_id=1, source_target_pairs={{0,2},{2,4},{4,6},{6,8},{8,10},{10,12},{12,14},{14,16},{16,18},{18... | collective-permute-start | bytes 786440 | tf_op jit(solution)/shard_map/ppermute | solution.py:124
  107.2 78.9 %copy-start.17 = (bf16[256,512]{1,0:T(8,128)(2,1)}, bf16[256,512]{1,0:T(8,128)(2,1)S(1)}, u32[]{:S(2)}) copy-start(bf16[256,512]{1,0:T(8,128)(2,1)S(1)} %collective-permute-done.7) | copy-start | bytes 786436
  107.2 43.6 %collective-permute-start.8 = (bf16[256,512]{1,0:T(8,128)(2,1)S(1)}, bf16[256,512]{1,0:T(8,128)(2,1)S(1)}, u32[]{:S(2)}, u32[]{:S(2)}) collective-permute-start(bf16[256,512]{1,0:T(8,128)(2,1)S(1)} %collective-permute-done.7), channel_id=1, source_target_pairs={{0,2},{2,4},{4,6},{6,8},{8,10},{10,12},{12,14},{14,16},{16,18},{18... | collective-permute-start | bytes 786440 | tf_op jit(solution)/shard_map/ppermute | solution.py:124
  150.8 12.0 %collective-permute-start.9 = (bf16[256,512]{1,0:T(8,128)(2,1)S(1)}, bf16[256,512]{1,0:T(8,128)(2,1)S(1)}, u32[]{:S(2)}, u32[]{:S(2)}) collective-permute-start(bf16[256,512]{1,0:T(8,128)(2,1)S(1)} %collective-permute-done.8), channel_id=1, source_target_pairs={{0,2},{2,4},{4,6},{6,8},{8,10},{10,12},{12,14},{14,16},{16,18},{18... | collective-permute-start | bytes 786440 | tf_op jit(solution)/shard_map/ppermute | solution.py:124
  153.6 22.7 %collective-permute-start = (bf16[16,512]{1,0:T(8,128)(2,1)S(1)}, bf16[16,512]{1,0:T(8,128)(2,1)S(1)}, u32[]{:S(2)}, u32[]{:S(2)}) collective-permute-start(bf16[16,512]{1,0:T(8,128)(2,1)S(1)} %slice.42), channel_id=1, source_target_pairs={{0,2},{2,4},{4,6},{6,8},{8,10},{10,12},{12,14},{14,16},{16,18},{18... | collective-permute-start | bytes 49160 | tf_op jit(solution)/shard_map/ppermute | solution.py:17
  162.8 12.6 %collective-permute-start.10 = (bf16[256,512]{1,0:T(8,128)(2,1)S(1)}, bf16[256,512]{1,0:T(8,128)(2,1)S(1)}, u32[]{:S(2)}, u32[]{:S(2)}) collective-permute-start(bf16[256,512]{1,0:T(8,128)(2,1)S(1)} %collective-permute-done.9), channel_id=1, source_target_pairs={{0,2},{2,4},{4,6},{6,8},{8,10},{10,12},{12,14},{14,16},{16,18},{18... | collective-permute-start | bytes 786440 | tf_op jit(solution)/shard_map/ppermute | solution.py:124
  175.4 10.7 %collective-permute-start.11 = (bf16[256,512]{1,0:T(8,128)(2,1)S(1)}, bf16[256,512]{1,0:T(8,128)(2,1)}, u32[]{:S(2)}, u32[]{:S(2)}) collective-permute-start(bf16[256,512]{1,0:T(8,128)(2,1)S(1)} %collective-permute-done.10), channel_id=1, source_target_pairs={{0,2},{2,4},{4,6},{6,8},{8,10},{10,12},{12,14},{14,16},{16,18},{18... | collective-permute-start | bytes 786440 | tf_op jit(solution)/shard_map/ppermute | solution.py:124
  186.1 10.3 %collective-permute-start.12 = (bf16[256,512]{1,0:T(8,128)(2,1)}, bf16[256,512]{1,0:T(8,128)(2,1)}, u32[]{:S(2)}, u32[]{:S(2)}) collective-permute-start(bf16[256,512]{1,0:T(8,128)(2,1)} %collective-permute-done.11), channel_id=1, source_target_pairs={{0,2},{2,4},{4,6},{6,8},{8,10},{10,12},{12,14},{14,16},{16,18},{18... | collective-permute-start | bytes 786440 | tf_op jit(solution)/shard_map/ppermute | solution.py:124
  196.4 10.2 %collective-permute-start.13 = (bf16[256,512]{1,0:T(8,128)(2,1)}, bf16[256,512]{1,0:T(8,128)(2,1)S(1)}, u32[]{:S(2)}, u32[]{:S(2)}) collective-permute-start(bf16[256,512]{1,0:T(8,128)(2,1)} %collective-permute-done.12), channel_id=1, source_target_pairs={{0,2},{2,4},{4,6},{6,8},{8,10},{10,12},{12,14},{14,16},{16,18},{18... | collective-permute-start | bytes 786440 | tf_op jit(solution)/shard_map/ppermute | solution.py:124
  196.4 36.5 %copy-start.14 = (bf16[256,512]{1,0:T(8,128)(2,1)S(1)}, bf16[256,512]{1,0:T(8,128)(2,1)}, u32[]{:S(2)}) copy-start(bf16[256,512]{1,0:T(8,128)(2,1)} %copy-done.13) | copy-start | bytes 786436
  196.4 36.5 %copy-start.12 = (bf16[256,512]{1,0:T(8,128)(2,1)S(1)}, bf16[256,512]{1,0:T(8,128)(2,1)}, u32[]{:S(2)}) copy-start(bf16[256,512]{1,0:T(8,128)(2,1)} %copy-done.11) | copy-start | bytes 786436
  196.6 36.4 %copy-start.8 = (bf16[256,512]{1,0:T(8,128)(2,1)S(1)}, bf16[256,512]{1,0:T(8,128)(2,1)}, u32[]{:S(2)}) copy-start(bf16[256,512]{1,0:T(8,128)(2,1)} %copy-done.7) | copy-start | bytes 786436
  196.6 36.4 %copy-start.6 = (bf16[256,512]{1,0:T(8,128)(2,1)S(1)}, bf16[256,512]{1,0:T(8,128)(2,1)}, u32[]{:S(2)}) copy-start(bf16[256,512]{1,0:T(8,128)(2,1)} %copy-done.5) | copy-start | bytes 786436
  196.6 36.4 %copy-start.4 = (bf16[256,512]{1,0:T(8,128)(2,1)S(1)}, bf16[256,512]{1,0:T(8,128)(2,1)}, u32[]{:S(2)}) copy-start(bf16[256,512]{1,0:T(8,128)(2,1)} %copy-done.3) | copy-start | bytes 786436
  206.6 10.4 %collective-permute-start.14 = (bf16[256,512]{1,0:T(8,128)(2,1)S(1)}, bf16[256,512]{1,0:T(8,128)(2,1)S(1)}, u32[]{:S(2)}, u32[]{:S(2)}) collective-permute-start(bf16[256,512]{1,0:T(8,128)(2,1)S(1)} %collective-permute-done.13), channel_id=1, source_target_pairs={{0,2},{2,4},{4,6},{6,8},{8,10},{10,12},{12,14},{14,16},{16,18},{18... | collective-permute-start | bytes 786440 | tf_op jit(solution)/shard_map/ppermute | solution.py:124
  216.9 10.0 %collective-permute-start.15 = (bf16[256,512]{1,0:T(8,128)(2,1)S(1)}, bf16[256,512]{1,0:T(8,128)(2,1)S(1)}, u32[]{:S(2)}, u32[]{:S(2)}) collective-permute-start(bf16[256,512]{1,0:T(8,128)(2,1)S(1)} %collective-permute-done.14), channel_id=1, source_target_pairs={{0,2},{2,4},{4,6},{6,8},{8,10},{10,12},{12,14},{14,16},{16,18},{18... | collective-permute-start | bytes 786440 | tf_op jit(solution)/shard_map/ppermute | solution.py:124
  (16 other events, 297.4 us)
Sparse Core Ops, SparseCore 0:
  8.9 11.7 all-gather.2
  81.2 89.1 all-gather.4
